TPU v7x, 512 devices: a whole 4x8x8 slice. The times are simulated.
512 devices in a mesh: fs: 64 (over z, y), tp: 8 (over x, core).
Axes of the slice: x: 4, y: 8, z: 8, core: 2. Of those that a mesh axis runs over, the one named last changes fastest.
Arguments:
- late_input: bfloat16 [8192, 2048], P('fs', 'tp'), may hold values from -6 to 6
- up_weight: bfloat16 [2048, 4096], P('tp', 'fs'), may hold values from -0.125 to 0.125
- down_weight: bfloat16 [4096, 2048], P('fs', 'tp'), may hold values from -0.09375 to 0.09375
- early_input: bfloat16 [8192, 2048], P('fs', 'tp'), may hold values from -6 to 6
- early_pre: bfloat16 [8192, 4096], P('fs'), may hold values from -6 to 6
- cotangent: bfloat16 [8192, 2048], P('fs', 'tp'), may hold values from -16 to 16
- up_sum: float32 [2048, 4096], P('tp', 'fs'), may hold values from -24 to 24
- down_sum: float32 [4096, 2048], P('fs', 'tp'), may hold values from -24 to 24
Outputs:
- late_pre: bfloat16 [8192, 4096], P('fs')
- late_out: bfloat16 [8192, 2048], P('fs', 'tp')
- input_grad: bfloat16 [8192, 2048], P('fs', 'tp')
- up_total: float32 [2048, 4096], P('tp', 'fs')
- down_total: float32 [4096, 2048], P('fs', 'tp')
All inputs are finite; a program needn't handle non-finite values.
Results may differ from a plain program's by a relative error of at most 0.025.
Values may be sent and summed in bfloat16 or wider, within the bound.
A program may use at most 128 MiB of HBM per device.

v0:
```python
import jax
import jax.numpy as jnp
from jax import lax
from jax.sharding import Mesh
from jax.sharding import PartitionSpec as P

FS = ("fs_0", "fs_1")


def gathered_total(shard, axis):
    parts = lax.all_gather(shard, axis).astype(jnp.float32)
    return parts.sum(axis=0)


def own_rows(so_far, axes):
    for axis in axes:
        so_far = lax.psum_scatter(so_far, axis, scatter_dimension=0, tiled=True)
    return so_far


def contract_rows(left, right):
    return lax.dot_general(
        left, right, (((0,), (0,)), ((), ())), preferred_element_type=jnp.float32
    )


def contract_cols(left, right):
    return lax.dot_general(
        left, right, (((1,), (1,)), ((), ())), preferred_element_type=jnp.float32
    )


def body(late_input, up_weight, down_weight, early_input, early_pre, cotangent, up_sum, down_sum):
    up_gathered = lax.all_gather(up_weight, FS, axis=1, tiled=True)
    down_gathered = lax.all_gather(down_weight, FS, axis=0, tiled=True)
    pre_terms = jnp.dot(late_input, up_gathered, preferred_element_type=jnp.float32)
    pre_summed = gathered_total(pre_terms.astype(jnp.bfloat16), "tp").astype(jnp.float32)
    late_pre = pre_summed.astype(jnp.bfloat16)
    late_hidden = jnp.square(jax.nn.relu(late_pre.astype(jnp.float32))).astype(jnp.bfloat16)
    early_float = early_pre.astype(jnp.float32)
    early_hidden = jnp.square(jax.nn.relu(early_float)).astype(jnp.bfloat16)
    late_out = jnp.dot(late_hidden, down_gathered, preferred_element_type=jnp.float32).astype(
        jnp.bfloat16
    )
    grad_terms = contract_cols(cotangent, down_gathered)
    hidden_grad = gathered_total(grad_terms.astype(jnp.bfloat16), "tp").astype(jnp.float32)
    pre_grad = (hidden_grad * 2.0 * jax.nn.relu(early_float)).astype(jnp.bfloat16)
    input_grad = contract_cols(pre_grad, up_gathered).astype(jnp.bfloat16)
    grad_local = lax.all_to_all(pre_grad, FS, split_axis=1, concat_axis=0, tiled=True)
    up_grad = contract_rows(lax.all_gather(early_input, FS, axis=0, tiled=True), grad_local)
    up_total = up_sum + up_grad
    down_grad = own_rows(contract_rows(early_hidden, cotangent), FS)
    down_total = down_sum + down_grad
    return (late_pre, late_out, input_grad, up_total, down_total)


def solution(mesh):
    split = Mesh(mesh.devices.reshape(8, 8, mesh.shape["tp"]), ("fs_0", "fs_1", "tp"))
    placed = (
        P(FS, "tp"),
        P("tp", FS),
        P(FS, "tp"),
        P(FS, "tp"),
        P(FS, None),
        P(FS, "tp"),
        P("tp", FS),
        P(FS, "tp"),
    )
    return jax.shard_map(
        body,
        mesh=split,
        in_specs=placed,
        out_specs=(P(FS, None), P(FS, "tp"), P(FS, "tp"), P("tp", FS), P(FS, "tp")),
        check_vma=False,
    )
```

profile of v0, /device:TPU:2, one launch (start us, length us, event | category | flops | bytes accessed | tf_op | source)
XLA Modules:
  0.0 414.4 jit_solution(17327344246205105072)
XLA Ops:
  8.0 0.0 copy-start
  8.0 0.0 all-gather.10.cloned.1.call-start
  8.1 0.7 all-gather.10.cloned.1.call-update
  8.7 0.0 reduce-scatter.3.cloned.1.call-start
  8.8 0.0 copy-done
  8.8 3.9 fusion.1
  12.8 0.0 reduce-scatter.3.cloned.1.call-update
  12.8 0.0 all-gather.8.cloned.1.call-start
  12.8 0.7 all-gather.8.cloned.1.call-update
  13.5 0.0 copy-start.6
  13.6 0.0 all-gather.16.cloned.1.call-start
  13.6 104.6 %all-gather.10.cloned.1.call-done = bf16[4096,256]{1,0:T(8,128)(2,1)} async-done(((bf16[64,256]{1,0:T(8,128)(2,1)}), bf16[4096,256]{1,0:T(8,128)(2,1)}) %all-gather.10.cloned.1.call-update) | async-done | bytes 2097168 | tf_op jit(solution)/shard_map/all_gather | solution.py:35
  118.2 3.5 convolution_convert_fusion
  121.6 0.0 all-gather.16.cloned.1.call-update
  121.6 0.0 reduce-scatter.5.cloned.1.call-start
  121.7 0.0 reduce-scatter.3.cloned.1.call-done
  121.7 0.5 reduce-scatter.5.cloned.1.call-update
  122.2 0.0 all-gather.14.cloned.1.call-start
  122.3 79.3 %all-gather.8.cloned.1.call-done = bf16[256,4096]{0,1:T(8,128)(2,1)} async-done(((bf16[256,64]{0,1:T(8,128)(2,1)}), bf16[256,4096]{0,1:T(8,128)(2,1)}) %all-gather.8.cloned.1.call-update) | async-done | bytes 2097168 | tf_op jit(solution)/shard_map/all_gather | solution.py:34
  201.6 0.0 copy-done.6
  201.6 3.4 convolution_convert_fusion.1
  204.9 0.0 all-gather.14.cloned.1.call-update
  205.0 0.0 all-gather.12.cloned.1.call-start
  205.0 0.5 all-gather.12.cloned.1.call-update
  205.6 49.1 %all-gather.16.cloned.1.call-done = bf16[1024,4096]{1,0:T(8,128)(2,1)} async-done(((bf16[128,4096]{1,0:T(8,128)(2,1)}), bf16[1024,4096]{1,0:T(8,128)(2,1)}) %all-gather.16.cloned.1.call-update) | async-done | bytes 8388624 | tf_op jit(solution)/shard_map/all_gather | solution.py:11
  254.7 0.0 copy-start.2
  254.7 5.1 %convert_reduce_fusion = f32[128,4096]{1,0:T(8,128)S(1)} fusion(bf16[8,128,4096]{2,1,0:T(8,128)(2,1)} %bitcast.25), kind=kLoop, calls=%fused_computation | loop fusion | flops 7864320 | bytes 10485760 | tf_op jit(solution)/shard_map/reduce_sum | solution.py:12
  259.9 0.0 copy-done.2
  259.9 0.3 multiply_convert_fusion.1
  260.2 0.0 copy-start.7
  260.2 1.3 copy.16
  261.5 13.5 %all-to-all-start = ((bf16[128,64,64]{0,2,1:T(8,128)(2,1)}), bf16[128,64,64]{0,2,1:T(8,128)(2,1)}, u32[]{:S(2)}, u32[]{:S(2)}) async-start(bf16[128,64,64]{0,2,1:T(8,128)(2,1)} %bitcast.2), calls=%async_computation | async-start | bytes 2097152 | tf_op jit(solution)/shard_map/all_to_all | solution.py:49
  275.1 0.0 reduce-scatter.5.cloned.1.call-done
  275.1 0.0 copy-done.7
  275.1 1.5 add.11
  276.6 35.9 %all-gather.14.cloned.1.call-done = bf16[1024,4096]{1,0:T(8,128)(2,1)} async-done(((bf16[128,4096]{1,0:T(8,128)(2,1)}), bf16[1024,4096]{1,0:T(8,128)(2,1)}) %all-gather.14.cloned.1.call-update) | async-done | bytes 8388624 | tf_op jit(solution)/shard_map/all_gather | solution.py:11
  312.5 0.0 copy-start.1
  312.5 6.2 %reduce_sum.21 = bf16[128,4096]{1,0:T(8,128)(2,1)} reduce(bf16[8,128,4096]{2,1,0:T(8,128)(2,1)} %bitcast.26, bf16[]{:T(256)} %constant.7.clone.1), dimensions={0}, to_apply=%region_0.0 | reduce | flops 3670016 | bytes 9437186 | tf_op jit(solution)/shard_map/reduce_sum | solution.py:12
  318.7 0.0 copy-done.1
  318.7 0.0 copy-start.3
  318.7 1.1 convolution_convert_fusion.2
  319.8 0.5 copy-done.3
  320.4 0.3 copy-done.4
  320.6 1.1 convolution_convert_fusion.3
  321.7 81.6 %all-gather.12.cloned.1.call-done = bf16[8192,256]{1,0:T(8,128)(2,1)} async-done(((bf16[128,256]{1,0:T(8,128)(2,1)}), bf16[8192,256]{1,0:T(8,128)(2,1)}) %all-gather.12.cloned.1.call-update) | async-done | bytes 4194320 | tf_op jit(solution)/shard_map/all_gather | solution.py:50
  403.3 0.0 all-to-all-done
  403.3 0.0 copy-done.5
  403.3 4.0 fusion
  (2 shorter events, 0.0 us)
Async XLA Ops:
  8.0 0.8 copy-start
  8.0 110.1 %all-gather.10.cloned.1.call-start = ((), (), s32[]{:S(2)}) async-start(), calls=%async_computation.4 | async-start | bytes 2129920 | tf_op jit(solution)/shard_map/all_gather | solution.py:35
  8.7 113.0 %reduce-scatter.3.cloned.1.call-start = ((), (), s32[]{:S(2)}) async-start(), calls=%async_computation.6 | async-start | bytes 4718592 | tf_op jit(solution)/shard_map/reduce_scatter | solution.py:17
  12.8 188.8 %all-gather.8.cloned.1.call-start = ((), (), s32[]{:S(2)}) async-start(), calls=%async_computation.3 | async-start | bytes 2129920 | tf_op jit(solution)/shard_map/all_gather | solution.py:34
  13.5 188.0 %copy-start.6 = (bf16[128,256]{1,0:T(8,128)(2,1)S(1)}, bf16[128,256]{1,0:T(8,128)(2,1)}, u32[]{:S(2)}) copy-start(bf16[128,256]{1,0:T(8,128)(2,1)} %param.8) | copy-start | bytes 196612
  13.6 241.2 %all-gather.16.cloned.1.call-start = ((), (), s32[]{:S(2)}) async-start(), calls=%async_computation.9 | async-start | bytes 9437184 | tf_op jit(solution)/shard_map/all_gather | solution.py:11
  121.6 153.5 %reduce-scatter.5.cloned.1.call-start = ((), (), s32[]{:S(2)}) async-start(), calls=%async_computation.7 | async-start | bytes 589824 | tf_op jit(solution)/shard_map/reduce_scatter | solution.py:17
  122.2 190.3 %all-gather.14.cloned.1.call-start = ((), (), s32[]{:S(2)}) async-start(), calls=%async_computation.8 | async-start | bytes 9437184 | tf_op jit(solution)/shard_map/all_gather | solution.py:11
  205.0 198.3 %all-gather.12.cloned.1.call-start = ((), (), s32[]{:S(2)}) async-start(), calls=%async_computation.5 | async-start | bytes 4259840 | tf_op jit(solution)/shard_map/all_gather | solution.py:50
  254.7 5.1 %copy-start.2 = (bf16[128,4096]{1,0:T(8,128)(2,1)S(1)}, bf16[128,4096]{1,0:T(8,128)(2,1)}, u32[]{:S(2)}) copy-start(bf16[128,4096]{1,0:T(8,128)(2,1)} %param.12) | copy-start | bytes 3145732
  260.2 14.9 %copy-start.7 = (f32[64,256]{1,0:T(8,128)S(1)}, f32[64,256]{1,0:T(8,128)}, u32[]{:S(2)}) copy-start(f32[64,256]{1,0:T(8,128)} %param.15) | copy-start | bytes 196612
  261.5 141.8 %all-to-all-start = ((bf16[128,64,64]{0,2,1:T(8,128)(2,1)}), bf16[128,64,64]{0,2,1:T(8,128)(2,1)}, u32[]{:S(2)}, u32[]{:S(2)}) async-start(bf16[128,64,64]{0,2,1:T(8,128)(2,1)} %bitcast.2), calls=%async_computation | async-start | bytes 2097152 | tf_op jit(solution)/shard_map/all_to_all | solution.py:49
  312.5 6.2 %copy-start.1 = (bf16[256,4096]{0,1:T(8,128)(2,1)S(1)}, bf16[256,4096]{0,1:T(8,128)(2,1)}, u32[]{:S(2)}) copy-start(bf16[256,4096]{0,1:T(8,128)(2,1)} %all-gather.8.cloned.1.call-done) | copy-start | bytes 6291460
  318.7 1.6 copy-start.3
  318.7 1.9 copy-start.4
  320.6 82.7 %copy-start.5 = (f32[256,64]{0,1:T(8,128)S(1)}, f32[256,64]{0,1:T(8,128)}, u32[]{:S(2)}) copy-start(f32[256,64]{0,1:T(8,128)} %param.14) | copy-start | bytes 196612
Sparse Core Ops, SparseCore 0:
  11.9 106.2 all-gather.9
  121.2 80.3 all-gather.7
  203.7 50.9 all-gather.15
  257.3 55.1 all-gather.13
  315.4 87.8 all-gather.11
Sparse Core Ops, SparseCore 1:
  12.9 64.5 reduce-scatter.2
  124.9 36.8 reduce-scatter.4
where the time goes:
time: 415 us; the launch traced here: 414 us
  waiting for transfers between devices  353 us (85%)
  matrix products  16.9 us (4%)
  between operations  15.3 us (4%)
  starting transfers between devices  13.8 us (3%)
  other arithmetic  13.2 us (3%)
    all_gather x1, waiting for transfers between devices, body(): down_gathered = lax.all_gather(down_weight, FS, axis=0, tiled=True)  105 us
    all_gather x2, waiting for transfers between devices, gathered_total(): parts = lax.all_gather(shard, axis).astype(jnp.float32)  85 us
    all_gather x1, waiting for transfers between devices, body(): lax.all_gather(early_input, FS, axis=0, tiled=True)  81.6 us
    all_gather x1, waiting for transfers between devices, body(): up_gathered = lax.all_gather(up_weight, FS, axis=1, tiled=True)  79.3 us
    all_to_all x1, starting transfers between devices, body(): lax.all_to_all(pre_grad, FS, split_axis=1, concat_axis=0, tiled=True)  13.5 us
    reduce_sum x2, other arithmetic, gathered_total(): return parts.sum(axis=0)  11.3 us
  transfers between devices with their start and end apart: 8, of which 5 were waited for; matrix products, arithmetic and copies ran while one was open for 7% of the time, Pallas kernels for 0%

commit v1 on v0

--- a/solution.py
+++ b/solution.py
@@ -47,7 +47,12 @@
     pre_grad = (hidden_grad * 2.0 * jax.nn.relu(early_float)).astype(jnp.bfloat16)
     input_grad = contract_cols(pre_grad, up_gathered).astype(jnp.bfloat16)
     grad_local = lax.all_to_all(pre_grad, FS, split_axis=1, concat_axis=0, tiled=True)
-    up_grad = contract_rows(lax.all_gather(early_input, FS, axis=0, tiled=True), grad_local)
+    up_grad = contract_rows(
+        jnp.concatenate(
+            lax.all_to_all(jnp.stack([early_input] * lax.axis_size(FS)), FS, 0, 0), axis=0
+        ),
+        grad_local,
+    )
     up_total = up_sum + up_grad
     down_grad = own_rows(contract_rows(early_hidden, cotangent), FS)
     down_total = down_sum + down_grad

time: 415 us -> 373 us (0.90)
  the two profiles are of different devices: /device:TPU:2 before, /device:TPU:8 now
where the time goes in v1:
time: 373 us
  waiting for transfers between devices  288 us (77%)
  starting transfers between devices  34.5 us (9%)
  matrix products  16.9 us (5%)
  between operations  15.3 us (4%)
  other arithmetic  13.1 us (4%)
  local copies, waits for them, and re-layouts  4.73 us (1%)
    all_gather x1, waiting for transfers between devices, body(): down_gathered = lax.all_gather(down_weight, FS, axis=0, tiled=True)  104 us
    all_gather x1, waiting for transfers between devices, body(): up_gathered = lax.all_gather(up_weight, FS, axis=1, tiled=True)  79.3 us
    all_to_all x1, waiting for transfers between devices, body(): lax.all_to_all(jnp.stack([early_input] * lax.axis_size(FS)), FS, 0, 0)  49.4 us
    all_gather x2, waiting for transfers between devices, gathered_total(): parts = lax.all_gather(shard, axis).astype(jnp.float32)  39 us
    all_to_all x1, starting transfers between devices, body(): lax.all_to_all(pre_grad, FS, split_axis=1, concat_axis=0, tiled=True)  24.7 us
    all_to_all x1, waiting for transfers between devices, body(): lax.all_to_all(pre_grad, FS, split_axis=1, concat_axis=0, tiled=True)  14.4 us
    reduce_sum x2, other arithmetic, gathered_total(): return parts.sum(axis=0)  11.3 us
    all_to_all x1, starting transfers between devices, body(): lax.all_to_all(jnp.stack([early_input] * lax.axis_size(FS)), FS, 0, 0)  9.51 us
  transfers between devices with their start and end apart: 8, of which 5 were waited for; matrix products, arithmetic and copies ran while one was open for 8% of the time, Pallas kernels for 0%

profile of v1, /device:TPU:8, one launch (start us, length us, event | category | flops | bytes accessed | tf_op | source)
XLA Modules:
  0.0 372.5 jit_solution(10098644241287315383)
XLA Ops:
  8.0 0.0 copy-start
  8.0 0.0 all-gather.9.cloned.1.call-start
  8.1 0.7 all-gather.9.cloned.1.call-update
  8.7 0.0 reduce-scatter.3.cloned.1.call-start
  8.8 0.0 copy-done
  8.8 3.9 %fusion.1 = f32[4096,256]{1,0:T(8,128)} fusion(bf16[128,256]{1,0:T(8,128)(2,1)S(1)} %copy-done, bf16[128,4096]{1,0:T(8,128)(2,1)} %param.12), kind=kOutput, calls=%fused_computation.11 | convolution fusion | flops 270532608 | bytes 5308416 | tf_op jit(solution)/shard_map/dot_general | solution.py:22
  12.8 0.0 reduce-scatter.3.cloned.1.call-update
  12.8 0.0 all-gather.7.cloned.1.call-start
  12.8 0.7 all-gather.7.cloned.1.call-update
  13.5 0.0 copy-start.7
  13.6 0.0 all-gather.13.cloned.1.call-start
  13.6 104.0 %all-gather.9.cloned.1.call-done = bf16[4096,256]{1,0:T(8,128)(2,1)} async-done(((bf16[64,256]{1,0:T(8,128)(2,1)}), bf16[4096,256]{1,0:T(8,128)(2,1)}) %all-gather.9.cloned.1.call-update) | async-done | bytes 2097168 | tf_op jit(solution)/shard_map/all_gather | solution.py:35
  117.6 3.4 convolution_convert_fusion
  121.0 0.0 all-gather.13.cloned.1.call-update
  121.0 0.0 reduce-scatter.5.cloned.1.call-start
  121.1 0.0 reduce-scatter.3.cloned.1.call-done
  121.1 0.5 reduce-scatter.5.cloned.1.call-update
  121.6 0.0 copy-start.5
  121.7 0.0 all-gather.11.cloned.1.call-start
  121.7 79.3 %all-gather.7.cloned.1.call-done = bf16[256,4096]{0,1:T(8,128)(2,1)} async-done(((bf16[256,64]{0,1:T(8,128)(2,1)}), bf16[256,4096]{0,1:T(8,128)(2,1)}) %all-gather.7.cloned.1.call-update) | async-done | bytes 2097168 | tf_op jit(solution)/shard_map/all_gather | solution.py:34
  201.0 0.0 copy-done.7
  201.0 3.4 convolution_convert_fusion.1
  204.4 0.0 all-gather.11.cloned.1.call-update
  204.4 0.0 copy-done.5
  204.4 2.5 stack.2
  206.9 9.5 %all-to-all-start.1 = ((bf16[64,128,256]{2,1,0:T(8,128)(2,1)}), bf16[64,128,256]{2,1,0:T(8,128)(2,1)}, u32[]{:S(2)}, u32[]{:S(2)}) async-start(bf16[64,128,256]{2,1,0:T(8,128)(2,1)} %stack.2), calls=%async_computation.1 | async-start | bytes 8388608 | tf_op jit(solution)/shard_map/all_to_all | solution.py:52
  216.4 39.0 %all-gather.13.cloned.1.call-done = bf16[1024,4096]{1,0:T(8,128)(2,1)} async-done(((bf16[128,4096]{1,0:T(8,128)(2,1)}), bf16[1024,4096]{1,0:T(8,128)(2,1)}) %all-gather.13.cloned.1.call-update) | async-done | bytes 8388624 | tf_op jit(solution)/shard_map/all_gather | solution.py:11
  255.4 0.0 copy-start.2
  255.4 5.1 %convert_reduce_fusion = f32[128,4096]{1,0:T(8,128)S(1)} fusion(bf16[8,128,4096]{2,1,0:T(8,128)(2,1)} %bitcast.22), kind=kLoop, calls=%fused_computation | loop fusion | flops 7864320 | bytes 10485760 | tf_op jit(solution)/shard_map/reduce_sum | solution.py:12
  260.5 0.0 copy-done.2
  260.6 0.3 multiply_convert_fusion.1
  260.9 0.0 copy-start.8
  260.9 1.4 copy.13
  262.2 49.4 %all-to-all-done.1 = bf16[64,128,256]{2,1,0:T(8,128)(2,1)} async-done(((bf16[64,128,256]{2,1,0:T(8,128)(2,1)}), bf16[64,128,256]{2,1,0:T(8,128)(2,1)}, u32[]{:S(2)}, u32[]{:S(2)}) %all-to-all-start.1) | async-done | bytes 4194336 | tf_op jit(solution)/shard_map/all_to_all | solution.py:52
  311.6 24.7 %all-to-all-start = ((bf16[128,64,64]{0,2,1:T(8,128)(2,1)}), bf16[128,64,64]{0,2,1:T(8,128)(2,1)}, u32[]{:S(2)}, u32[]{:S(2)}) async-start(bf16[128,64,64]{0,2,1:T(8,128)(2,1)} %bitcast.2), calls=%async_computation | async-start | bytes 2097152 | tf_op jit(solution)/shard_map/all_to_all | solution.py:49
  336.3 0.0 reduce-scatter.5.cloned.1.call-done
  336.4 0.0 copy-done.8
  336.4 1.5 add.11
  337.8 0.0 all-gather.11.cloned.1.call-done
  337.8 6.2 %reduce_sum.21 = bf16[128,4096]{1,0:T(8,128)(2,1)} reduce(bf16[8,128,4096]{2,1,0:T(8,128)(2,1)} %bitcast.23, bf16[]{:T(256)} %constant.7.clone.1), dimensions={0}, to_apply=%region_0.0 | reduce | flops 3670016 | bytes 9437186 | tf_op jit(solution)/shard_map/reduce_sum | solution.py:12
  344.0 0.0 copy-done.1
  344.1 1.1 convolution_convert_fusion.2
  345.1 0.5 copy-done.3
  345.7 0.3 copy-done.4
  345.9 1.1 convolution_convert_fusion.3
  347.0 14.4 %all-to-all-done = bf16[128,64,64]{0,2,1:T(8,128)(2,1)} async-done(((bf16[128,64,64]{0,2,1:T(8,128)(2,1)}), bf16[128,64,64]{0,2,1:T(8,128)(2,1)}, u32[]{:S(2)}, u32[]{:S(2)}) %all-to-all-start) | async-done | bytes 1048608 | tf_op jit(solution)/shard_map/all_to_all | solution.py:49
  361.4 0.0 copy-done.6
  361.4 4.0 %fusion = f32[256,64]{0,1:T(8,128)} fusion(f32[256,64]{0,1:T(8,128)S(1)} %copy-done.6, bf16[64,128,256]{2,1,0:T(8,128)(2,1)} %all-to-all-done.1, bf16[128,64,64]{0,2,1:T(8,128)(2,1)} %all-to-all-done), kind=kOutput, calls=%fused_computation.10 | convolution fusion | flops 268451840 | bytes 5373952 | tf_op jit(solution)/shard_map/dot_general | solution.py:22
  (4 shorter events, 0.0 us)
Async XLA Ops:
  8.0 0.8 copy-start
  8.0 109.6 %all-gather.9.cloned.1.call-start = ((), (), s32[]{:S(2)}) async-start(), calls=%async_computation.5 | async-start | bytes 2129920 | tf_op jit(solution)/shard_map/all_gather | solution.py:35
  8.7 112.4 %reduce-scatter.3.cloned.1.call-start = ((), (), s32[]{:S(2)}) async-start(), calls=%async_computation.6 | async-start | bytes 4718592 | tf_op jit(solution)/shard_map/reduce_scatter | solution.py:17
  12.8 188.2 %all-gather.7.cloned.1.call-start = ((), (), s32[]{:S(2)}) async-start(), calls=%async_computation.4 | async-start | bytes 2129920 | tf_op jit(solution)/shard_map/all_gather | solution.py:34
  13.5 187.4 %copy-start.7 = (bf16[128,256]{1,0:T(8,128)(2,1)S(1)}, bf16[128,256]{1,0:T(8,128)(2,1)}, u32[]{:S(2)}) copy-start(bf16[128,256]{1,0:T(8,128)(2,1)} %param.8) | copy-start | bytes 196612
  13.6 241.8 %all-gather.13.cloned.1.call-start = ((), (), s32[]{:S(2)}) async-start(), calls=%async_computation.9 | async-start | bytes 9437184 | tf_op jit(solution)/shard_map/all_gather | solution.py:11
  121.0 215.3 %reduce-scatter.5.cloned.1.call-start = ((), (), s32[]{:S(2)}) async-start(), calls=%async_computation.7 | async-start | bytes 589824 | tf_op jit(solution)/shard_map/reduce_scatter | solution.py:17
  121.6 82.7 %copy-start.5 = (bf16[128,256]{1,0:T(8,128)(2,1)S(1)}, bf16[128,256]{1,0:T(8,128)(2,1)}, u32[]{:S(2)}) copy-start(bf16[128,256]{1,0:T(8,128)(2,1)} %param.11) | copy-start | bytes 196612
  121.7 216.2 %all-gather.11.cloned.1.call-start = ((), (), s32[]{:S(2)}) async-start(), calls=%async_computation.8 | async-start | bytes 9437184 | tf_op jit(solution)/shard_map/all_gather | solution.py:11
  206.9 104.7 %all-to-all-start.1 = ((bf16[64,128,256]{2,1,0:T(8,128)(2,1)}), bf16[64,128,256]{2,1,0:T(8,128)(2,1)}, u32[]{:S(2)}, u32[]{:S(2)}) async-start(bf16[64,128,256]{2,1,0:T(8,128)(2,1)} %stack.2), calls=%async_computation.1 | async-start | bytes 8388608 | tf_op jit(solution)/shard_map/all_to_all | solution.py:52
  255.4 5.1 %copy-start.2 = (bf16[128,4096]{1,0:T(8,128)(2,1)S(1)}, bf16[128,4096]{1,0:T(8,128)(2,1)}, u32[]{:S(2)}) copy-start(bf16[128,4096]{1,0:T(8,128)(2,1)} %param.12) | copy-start | bytes 3145732
  260.9 75.5 %copy-start.8 = (f32[64,256]{1,0:T(8,128)S(1)}, f32[64,256]{1,0:T(8,128)}, u32[]{:S(2)}) copy-start(f32[64,256]{1,0:T(8,128)} %param.15) | copy-start | bytes 196612
  311.6 49.8 %all-to-all-start = ((bf16[128,64,64]{0,2,1:T(8,128)(2,1)}), bf16[128,64,64]{0,2,1:T(8,128)(2,1)}, u32[]{:S(2)}, u32[]{:S(2)}) async-start(bf16[128,64,64]{0,2,1:T(8,128)(2,1)} %bitcast.2), calls=%async_computation | async-start | bytes 2097152 | tf_op jit(solution)/shard_map/all_to_all | solution.py:49
  337.8 6.2 %copy-start.1 = (bf16[256,4096]{0,1:T(8,128)(2,1)S(1)}, bf16[256,4096]{0,1:T(8,128)(2,1)}, u32[]{:S(2)}) copy-start(bf16[256,4096]{0,1:T(8,128)(2,1)} %all-gather.7.cloned.1.call-done) | copy-start | bytes 6291460
  344.0 1.6 copy-start.3
  344.1 1.9 copy-start.4
  345.9 15.5 %copy-start.6 = (f32[256,64]{0,1:T(8,128)S(1)}, f32[256,64]{0,1:T(8,128)}, u32[]{:S(2)}) copy-start(f32[256,64]{0,1:T(8,128)} %param.14) | copy-start | bytes 196612
Sparse Core Ops, SparseCore 0:
  11.9 105.6 all-gather.8
  120.7 80.2 all-gather.6
  203.1 52.2 all-gather.12
  258.0 55.1 all-gather.10
Sparse Core Ops, SparseCore 1:
  12.9 64.4 reduce-scatter.2
  124.3 36.9 reduce-scatter.4
